TPU v7x, 512 devices: a whole 4x4x16 slice. The times are simulated.
512 devices in a mesh: gr: 2 (over z_hi), fs: 32 (over z_lo, y), tp: 8 (over x, core).
Axes of the slice: x: 4, y: 4, z: 16 (z_hi: 2, z_lo: 8; z = z_hi * 8 + z_lo), core: 2. Of those that a mesh axis runs over, the one named last changes fastest.
Arguments:
- tokens: bfloat16 [24576, 2048], P(('gr', 'fs')), may hold values from -6 to 6
- route_ids: int32 [24576, 2], P(('gr', 'fs')), may hold values from 0 to 31, as said below
- route_weights: float32 [24576, 2], P(('gr', 'fs')), may hold values from 0.1 to 1
- norm_gain: float32 [2048], P(('gr', 'fs')), may hold values from 0.1 to 1.9
- gate_weight: float32 [32, 2048, 1024], P(None, ('gr', 'fs'), 'tp'), may hold values from -0.125 to 0.125
- up_weight: float32 [32, 2048, 1024], P(None, ('gr', 'fs'), 'tp'), may hold values from -0.125 to 0.125
- down_weight: float32 [32, 1024, 2048], P(None, ('gr', 'fs'), 'tp'), may hold values from -0.1875 to 0.1875
Outputs:
- gate_new: bfloat16 [32, 2048, 1024], P('fs', None, 'tp')
- up_new: bfloat16 [32, 2048, 1024], P('fs', None, 'tp')
- down_new: bfloat16 [32, 1024, 2048], P('fs', 'tp')
- mixed: bfloat16 [24576, 2048], P(('gr', 'fs'), 'tp')
Inputs may be any that keep to these rules, and one draw needn't show every extreme that they name: `route_ids`: each row names two different experts of one group (expert e belongs to group e // 8); in each device's block of 384 rows every expert is named by exactly 24 rows.
All inputs are finite; a program needn't handle non-finite values.
Results may differ from a plain program's by a relative error of at most 0.015.
Values may be sent and summed in bfloat16 or wider, within the bound.
A program may use at most 64 MiB of HBM per device.

v0:
```python
import jax
import jax.numpy as jnp
from jax import lax
from jax.sharding import Mesh
from jax.sharding import PartitionSpec as P

TP = ("tp_0", "tp_1")


def side_by_side(arrays, axis, split_dim, concat_dim, along):
    ends, at = ([], 0)
    for a in arrays[:-1]:
        at += a.shape[along]
        ends.append(at)
    both = jnp.concatenate(arrays, axis=along)
    return tuple(
        jnp.split(
            lax.all_to_all(both, axis, split_axis=split_dim, concat_axis=concat_dim, tiled=True),
            ends,
            axis=along,
        )
    )


def in_one_piece(arrays, axis, dim, along):
    ends, at = ([], 0)
    for a in arrays[:-1]:
        at += a.shape[along]
        ends.append(at)
    both = jnp.concatenate(arrays, axis=along)
    return tuple(jnp.split(lax.all_gather(both, axis, axis=dim, tiled=True), ends, axis=along))


def split_up(array, dim, devices):
    before, after = (array.shape[:dim], array.shape[dim + 1 :])
    return jnp.moveaxis(array.reshape(*before, devices, -1, *after), dim, 0)


def laid_out(pieces, dim):
    pieces = jnp.moveaxis(pieces, 0, dim)
    lengths = pieces.shape
    return pieces.reshape(*lengths[:dim], lengths[dim] * lengths[dim + 1], *lengths[dim + 2 :])


def exchange_in_order(pieces, axes, turns):
    inside = pieces.shape[1:]
    whole = pieces.reshape(*(lax.axis_size(a) for a in axes), *inside)
    for k in turns:
        whole = lax.all_to_all(whole, axes[k], k, k, tiled=True)
    return whole.reshape(-1, *inside)


def exchange_by_axis(array, axes, turns, split_dim, concat_dim):
    pieces = split_up(array, split_dim, lax.axis_size(axes))
    return laid_out(exchange_in_order(pieces, axes, turns), concat_dim)


def local(tokens, route_ids, route_weights, norm_gain, gate_weight, up_weight, down_weight):
    gate_folded = (gate_weight * norm_gain[None, :, None]).astype(jnp.bfloat16)
    up_folded = (up_weight * norm_gain[None, :, None]).astype(jnp.bfloat16)
    down_rounded = down_weight.astype(jnp.bfloat16)
    moved = (
        *side_by_side((gate_folded, up_folded), "fs", 0, 1, 2),
        lax.all_to_all(down_rounded, "fs", split_axis=0, concat_axis=1, tiled=True),
    )
    gate_new, up_new, down_whole = (
        *in_one_piece((moved[0], moved[1]), "gr", 1, 0),
        lax.all_gather(moved[2], "gr", axis=1, tiled=True),
    )
    down_new = exchange_by_axis(down_whole, TP, (1, 0), 1, 2)
    tok = tokens.shape[0]
    width = tokens.shape[1]
    experts = gate_weight.shape[0]
    cap = 2 * tok // experts
    flat_ids = route_ids.reshape(-1)
    onehot = (flat_ids[:, None] == jnp.arange(experts, dtype=jnp.int32)[None, :]).astype(jnp.int32)
    slot = jnp.sum(jnp.cumsum(onehot, axis=0) * onehot, axis=1) - 1
    position = flat_ids * cap + slot
    source = (
        jnp.zeros((experts * cap,), jnp.int32)
        .at[position]
        .set(jnp.arange(2 * tok, dtype=jnp.int32) // 2)
    )
    widened = tokens.astype(jnp.float32)
    normed = (
        widened * lax.rsqrt(jnp.mean(widened * widened, axis=-1, keepdims=True) + 1e-06)
    ).astype(jnp.bfloat16)
    outgoing = normed[source].reshape(experts, cap, width)
    received = lax.all_to_all(outgoing, "fs", split_axis=0, concat_axis=0, tiled=True)
    senders, count, _ = received.shape
    rows = received.reshape(senders * count, width)
    first = jnp.dot(rows, gate_new[0], preferred_element_type=jnp.float32)
    second = jnp.dot(rows, up_new[0], preferred_element_type=jnp.float32)
    hidden = (jax.nn.silu(first) * second).astype(jnp.bfloat16)
    hidden_width = hidden.shape[1]
    down_local = down_whole[0]
    out_columns = down_local.shape[1]
    row_count = hidden.shape[0]
    piece = lax.all_gather(hidden, TP, axis=1, tiled=True)
    piece_width = piece.shape[1]
    blocks = piece_width // hidden_width
    partials = jnp.einsum(
        "mbf,bfd->bmd",
        piece.reshape(row_count, blocks, hidden_width),
        down_local.reshape(blocks, hidden_width, out_columns),
        preferred_element_type=jnp.float32,
    ).astype(jnp.bfloat16)
    total = jnp.sum(partials.astype(jnp.float32), axis=0)
    summed = total.reshape(senders, count, out_columns)
    returned = lax.all_to_all(
        summed.astype(jnp.bfloat16), "fs", split_axis=0, concat_axis=0, tiled=True
    )
    columns = returned.shape[2]
    route_out = returned.reshape(experts * cap, columns)[position].reshape(tok, 2, columns)
    mixed = jnp.sum(route_weights[:, :, None] * route_out.astype(jnp.float32), axis=1).astype(
        jnp.bfloat16
    )
    return (gate_new, up_new, down_new, mixed)


def solution(mesh):
    torus = Mesh(
        mesh.devices.reshape(mesh.shape["gr"], mesh.shape["fs"], 4, 2), ("gr", "fs", "tp_0", "tp_1")
    )
    placed = (
        P(("gr", "fs"), None),
        P(("gr", "fs"), None),
        P(("gr", "fs"), None),
        P(("gr", "fs")),
        P(None, ("gr", "fs"), TP),
        P(None, ("gr", "fs"), TP),
        P(None, ("gr", "fs"), TP),
    )
    return jax.shard_map(
        local,
        mesh=torus,
        in_specs=placed,
        out_specs=(P("fs", None, TP), P("fs", None, TP), P("fs", TP, None), P(("gr", "fs"), TP)),
        check_vma=False,
    )
```

profile of v0, /device:TPU:1, one launch (start us, length us, event | category | flops | bytes accessed | tf_op | source)
XLA Modules:
  0.0 368.0 jit_solution(3223288350482646378)
XLA Ops:
  7.2 0.0 copy-start.2
  7.2 0.0 copy-start
  7.2 1.5 multiply_convert_fusion.1
  8.7 0.9 pad_maximum_fusion
  9.6 16.2 %all-to-all-start = ((bf16[32,32,256]{2,1,0:T(8,128)(2,1)}), bf16[32,32,256]{2,1,0:T(8,128)(2,1)}, u32[]{:S(2)}, u32[]{:S(2)}) async-start(bf16[32,32,256]{2,1,0:T(8,128)(2,1)} %pad_maximum_fusion), calls=%async_computation | async-start | bytes 1048576 | tf_op jit(solution)/shard_map/all_to_all | solution.py:18
  25.8 0.0 copy-done.2
  25.8 0.1 copy.34
  25.9 0.1 eq.29
  26.1 0.1 eq.25
  26.2 1.7 reduce-window.6
  28.0 0.3 slice_reduce_fusion
  28.3 0.1 copy.33
  28.4 0.2 mul.68
  28.6 0.1 fusion.9
  28.7 3.4 scatter_custom_fusion
  32.2 0.0 copy-done
  32.2 0.4 fusion
  32.6 0.3 fusion.1
  32.9 4.3 %gather_fusion = bf16[768,2048]{1,0:T(8,128)(2,1)} fusion(bf16[384,2048]{1,0:T(8,128)(2,1)S(1)} %fusion.1, s32[1024]{0:T(1024)S(1)} %pad_clamp_fusion.1), kind=kCustom, calls=%fused_computation | custom fusion | bytes 6294528 | tf_op jit(solution)/shard_map/gather | solution.py:88
  37.2 15.3 %all-to-all-done = bf16[32,32,256]{2,1,0:T(8,128)(2,1)} async-done(((bf16[32,32,256]{2,1,0:T(8,128)(2,1)}), bf16[32,32,256]{2,1,0:T(8,128)(2,1)}, u32[]{:S(2)}, u32[]{:S(2)}) %all-to-all-start) | async-done | bytes 524320 | tf_op jit(solution)/shard_map/all_to_all | solution.py:18
  52.5 8.8 %all-to-all-start.4 = ((bf16[32,24,2048]{2,1,0:T(8,128)(2,1)}), bf16[32,24,2048]{2,1,0:T(8,128)(2,1)S(1)}, u32[]{:S(2)}, u32[]{:S(2)}) async-start(bf16[32,24,2048]{2,1,0:T(8,128)(2,1)} %bitcast.48), calls=%async_computation.4 | async-start | bytes 6291456 | tf_op jit(solution)/shard_map/all_to_all | solution.py:89
  61.3 0.0 all-gather.3.cloned.1.call-start
  61.3 1.1 fusion.18
  62.4 0.8 pad_maximum_fusion.1
  63.2 0.0 all-gather.3.cloned.1.call-update
  63.3 0.0 all-gather.5.cloned.1.call-start
  63.3 67.4 %all-gather.3.cloned.1.call-done = bf16[2,2048,128]{2,1,0:T(8,128)(2,1)} async-done(((bf16[2,1024,128]{2,1,0:T(8,128)(2,1)}), bf16[2,2048,128]{2,1,0:T(8,128)(2,1)}) %all-gather.3.cloned.1.call-update) | async-done | bytes 1048592 | tf_op jit(solution)/shard_map/all_gather | solution.py:31
  130.7 2.2 fusion.17
  132.9 112.7 %all-to-all-done.4 = bf16[32,24,2048]{2,1,0:T(8,128)(2,1)S(1)} async-done(((bf16[32,24,2048]{2,1,0:T(8,128)(2,1)}), bf16[32,24,2048]{2,1,0:T(8,128)(2,1)S(1)}, u32[]{:S(2)}, u32[]{:S(2)}) %all-to-all-start.4) | async-done | bytes 3145760 | tf_op jit(solution)/shard_map/all_to_all | solution.py:89
  245.6 2.1 fusion.6
  247.7 1.7 fusion.4
  249.4 0.0 all-gather.5.cloned.1.call-update
  249.4 1.1 convert_element_type.42
  250.5 25.1 %all_to_all.44 = bf16[32,16,256]{2,1,0:T(8,128)(2,1)S(1)} all-to-all(bf16[32,16,256]{2,1,0:T(8,128)(2,1)S(1)} %convert_element_type.42), channel_id=1, replica_groups=mesh['gr'=2,'fs'=32,'tp_0'=4,'tp_1'=2] {'fs'}, dimensions={0} | all-to-all | bytes 524288 | tf_op jit(solution)/shard_map/all_to_all | solution.py:64
  275.6 23.8 %all_gather.10 = bf16[1,1024,256]{2,1,0:T(8,128)(2,1)S(1)} all-gather(bf16[1,512,256]{2,1,0:T(8,128)(2,1)S(1)} %bitcast.52), channel_id=1, replica_groups=mesh['gr'=2,'fs'=32,'tp_0'=4,'tp_1'=2] {'gr'}, dimensions={1}, use_global_device_ids=true | all-gather | bytes 786432 | tf_op jit(solution)/shard_map/all_gather | solution.py:68
  299.4 13.2 %all_to_all.45 = bf16[4,2,1,128,256]{4,3,0,2,1:T(8,128)(2,1)S(1)} all-to-all(bf16[4,2,1,128,256]{4,3,0,2,1:T(8,128)(2,1)S(1)} %copy.29), channel_id=1, replica_groups=mesh['gr'=2,'fs'=32,'tp_0'=4,'tp_1'=2] {'tp_1'}, dimensions={1} | all-to-all | bytes 1048576 | tf_op jit(solution)/shard_map/all_to_all | solution.py:49
  312.6 0.8 copy.30
  313.4 4.2 %all-to-all-start.3 = ((bf16[4,2,1,128,256]{4,3,1,2,0:T(8,128)(2,1)}), bf16[4,2,1,128,256]{4,3,1,2,0:T(8,128)(2,1)S(1)}, u32[]{:S(2)}, u32[]{:S(2)}) async-start(bf16[4,2,1,128,256]{4,3,1,2,0:T(8,128)(2,1)} %copy.30), calls=%async_computation.3 | async-start | bytes 1048576 | tf_op jit(solution)/shard_map/all_to_all | solution.py:49
  317.6 3.2 convert_reduce_fusion
  320.8 5.7 %all-to-all-done.3 = bf16[4,2,1,128,256]{4,3,1,2,0:T(8,128)(2,1)S(1)} async-done(((bf16[4,2,1,128,256]{4,3,1,2,0:T(8,128)(2,1)}), bf16[4,2,1,128,256]{4,3,1,2,0:T(8,128)(2,1)S(1)}, u32[]{:S(2)}, u32[]{:S(2)}) %all-to-all-start.3) | async-done | bytes 524320 | tf_op jit(solution)/shard_map/all_to_all | solution.py:49
  326.5 9.7 %all-to-all-start.5 = ((bf16[32,24,256]{2,1,0:T(8,128)(2,1)}), bf16[32,24,256]{2,1,0:T(8,128)(2,1)S(1)}, u32[]{:S(2)}, u32[]{:S(2)}) async-start(bf16[32,24,256]{2,1,0:T(8,128)(2,1)} %bitcast.11), calls=%async_computation.5 | async-start | bytes 786432 | tf_op jit(solution)/shard_map/all_to_all | solution.py:110
  336.2 0.0 copy-done.3
  336.2 0.1 copy.32
  336.4 0.8 copy.39
  337.2 19.1 %all-to-all-done.5 = bf16[32,24,256]{2,1,0:T(8,128)(2,1)S(1)} async-done(((bf16[32,24,256]{2,1,0:T(8,128)(2,1)}), bf16[32,24,256]{2,1,0:T(8,128)(2,1)S(1)}, u32[]{:S(2)}, u32[]{:S(2)}) %all-to-all-start.5) | async-done | bytes 393248 | tf_op jit(solution)/shard_map/all_to_all | solution.py:110
  356.4 2.6 gather_fusion.1
  359.0 0.4 reshape.105
  359.4 1.7 multiply_reduce_fusion
  (15 shorter events, 0.1 us)
Async XLA Ops:
  7.2 18.6 %copy-start.2 = (s32[384,2]{0,1:T(2,128)S(1)}, s32[384,2]{0,1:T(2,128)}, u32[]{:S(2)}) copy-start(s32[384,2]{0,1:T(2,128)} %param.8) | copy-start | bytes 9220
  7.2 25.0 %copy-start = (bf16[384,2048]{1,0:T(8,128)(2,1)S(1)}, bf16[384,2048]{1,0:T(8,128)(2,1)}, u32[]{:S(2)}) copy-start(bf16[384,2048]{1,0:T(8,128)(2,1)} %param.7) | copy-start | bytes 4718596
  9.6 42.9 %all-to-all-start = ((bf16[32,32,256]{2,1,0:T(8,128)(2,1)}), bf16[32,32,256]{2,1,0:T(8,128)(2,1)}, u32[]{:S(2)}, u32[]{:S(2)}) async-start(bf16[32,32,256]{2,1,0:T(8,128)(2,1)} %pad_maximum_fusion), calls=%async_computation | async-start | bytes 1048576 | tf_op jit(solution)/shard_map/all_to_all | solution.py:18
  52.5 193.1 %all-to-all-start.4 = ((bf16[32,24,2048]{2,1,0:T(8,128)(2,1)}), bf16[32,24,2048]{2,1,0:T(8,128)(2,1)S(1)}, u32[]{:S(2)}, u32[]{:S(2)}) async-start(bf16[32,24,2048]{2,1,0:T(8,128)(2,1)} %bitcast.48), calls=%async_computation.4 | async-start | bytes 6291456 | tf_op jit(solution)/shard_map/all_to_all | solution.py:89
  61.3 69.4 %all-gather.3.cloned.1.call-start = ((), (), s32[]{:S(2)}) async-start(), calls=%async_computation.6 | async-start | bytes 1572864 | tf_op jit(solution)/shard_map/all_gather | solution.py:31
  63.3 254.3 %all-gather.5.cloned.1.call-start = ((), (), s32[]{:S(2)}) async-start(), calls=%async_computation.7 | async-start | bytes 1769472 | tf_op jit(solution)/shard_map/all_gather | solution.py:99
  245.6 2.1 copy-start.1
  313.4 22.8 %copy-start.3 = (f32[384,2]{0,1:T(2,128)S(1)}, f32[384,2]{0,1:T(2,128)}, u32[]{:S(2)}) copy-start(f32[384,2]{0,1:T(2,128)} %param.9) | copy-start | bytes 9220
  313.4 13.1 %all-to-all-start.3 = ((bf16[4,2,1,128,256]{4,3,1,2,0:T(8,128)(2,1)}), bf16[4,2,1,128,256]{4,3,1,2,0:T(8,128)(2,1)S(1)}, u32[]{:S(2)}, u32[]{:S(2)}) async-start(bf16[4,2,1,128,256]{4,3,1,2,0:T(8,128)(2,1)} %copy.30), calls=%async_computation.3 | async-start | bytes 1048576 | tf_op jit(solution)/shard_map/all_to_all | solution.py:49
  326.5 29.8 %all-to-all-start.5 = ((bf16[32,24,256]{2,1,0:T(8,128)(2,1)}), bf16[32,24,256]{2,1,0:T(8,128)(2,1)S(1)}, u32[]{:S(2)}, u32[]{:S(2)}) async-start(bf16[32,24,256]{2,1,0:T(8,128)(2,1)} %bitcast.11), calls=%async_computation.5 | async-start | bytes 786432 | tf_op jit(solution)/shard_map/all_to_all | solution.py:110
Sparse Core Ops, SparseCore 0:
  64.8 65.8 all-gather.2
  249.5 31.3 all-gather.4
where the time goes:
time: 371 us; the launch traced here: 368 us
  waiting for transfers between devices  220 us (59%)
  blocking collectives  62.1 us (17%)
  starting transfers between devices  38.9 us (10%)
  local copies, waits for them, and re-layouts  16.8 us (5%)
  between operations  14.3 us (4%)
  other arithmetic  8.64 us (2%)
  matrix products  6.93 us (2%)
    all_to_all x1, waiting for transfers between devices, local(): lax.all_to_all(outgoing, 'fs', split_axis=0, concat_axis=0, tiled=True)  113 us
    all_gather x1, waiting for transfers between devices, in_one_piece(): lax.all_gather(both, axis, axis=dim, tiled=True)  67.4 us
    all_to_all x1, blocking collectives, local(): lax.all_to_all(down_rounded, 'fs', split_axis=0, concat_axis=1, tiled=True)  25.1 us
    all_gather x1, blocking collectives, local(): lax.all_gather(moved[2], 'gr', axis=1, tiled=True)  23.8 us
    all_to_all x1, waiting for transfers between devices, local(): lax.all_to_all(summed.astype(jnp.bfloat16), 'fs', split_axis=0, concat_ax...  19.1 us
    all_to_all x1, starting transfers between devices, side_by_side(): lax.all_to_all(both, axis, split_axis=split_dim, concat_axis=concat_dim,...  16.2 us
    all_to_all x1, waiting for transfers between devices, side_by_side(): lax.all_to_all(both, axis, split_axis=split_dim, concat_axis=concat_dim,...  15.3 us
    all_to_all x1, blocking collectives, exchange_in_order(): whole = lax.all_to_all(whole, axes[k], k, k, tiled=True)  13.2 us
  transfers between devices with their start and end apart: 6, of which 5 were waited for; matrix products, arithmetic and copies ran while one was open for 6% of the time, Pallas kernels for 0%

commit v1 on v0

v1 whole, which is shorter than its diff:
```python
import jax
import jax.numpy as jnp
from jax import lax
from jax.experimental import pallas as pl
from jax.experimental.pallas import tpu as pltpu
from jax.sharding import Mesh
from jax.sharding import PartitionSpec as P

MESH = pl.DeviceIdType.MESH
BF, F32 = jnp.bfloat16, jnp.float32
NZ, NH, NL, NY, NX, NC = 16, 2, 8, 4, 4, 2
NTP = NX * NC
TOK, WIDTH, CAP, EXP = 384, 2048, 24, 32
WCOL = WIDTH // NTP
ROWS = EXP * CAP


def halves_down(v):
    return jnp.concatenate([v[:, :, :128], v[:, :, 128:]], axis=1)


def kernel(
    tokens, idsc, idsr, wts, gain, gate, up, down,
    gate_out, up_out, down_out, mixed,
    ws, yw, gw, ds, yd, dw, dn, ts, yt, xa, xr, hh, os_, rz, rt, rr, q0, q1,
    y_send, y_recv, z_send, z_recv, x_send, x_recv, b_send, b_recv, c_sem, loc, out_sem,
):
    zh, zl, my = lax.axis_index("zh"), lax.axis_index("zl"), lax.axis_index("y")
    mx, mc = lax.axis_index("x"), lax.axis_index("c")
    zz = zh * NL + zl
    tp = mx * NC + mc

    def at_z(z):
        z = (z + 2 * NZ) % NZ
        return {"zh": z // NL, "zl": z % NL}

    def copy_to(src, dst, send, recv, dev):
        return pltpu.make_async_remote_copy(
            src_ref=src, dst_ref=dst, send_sem=send, recv_sem=recv, device_id=dev, device_id_type=MESH
        )

    def wait_bytes(ref, sem):
        pltpu.make_async_copy(ref, ref, sem).wait()

    bar = pltpu.get_barrier_semaphore()

    @pl.loop(1, NY)
    def _(d):
        pl.semaphore_signal(bar, inc=1, device_id={"y": (my + d) % NY}, device_id_type=MESH)

    @pl.loop(1, NZ)
    def _(d):
        pl.semaphore_signal(bar, inc=1, device_id=at_z(zz + d), device_id_type=MESH)

    @pl.loop(1, NTP)
    def _(d):
        t = (tp + d) % NTP
        pl.semaphore_signal(bar, inc=1, device_id={"x": t // NC, "c": t % NC}, device_id_type=MESH)

    def relabel(e):
        return (e % NY) * NL + e // NY

    first_r, second_r = relabel(idsr[0:1, :]), relabel(idsr[1:2, :])
    ex = lax.broadcasted_iota(jnp.int32, (EXP, TOK), 0)
    member_r = (ex == first_r) | (ex == second_r)
    a = lax.broadcasted_iota(jnp.int32, (TOK, TOK), 0)
    b = lax.broadcasted_iota(jnp.int32, (TOK, TOK), 1)
    before = (a < b).astype(F32).astype(BF)
    rank_r = jnp.dot(member_r.astype(F32).astype(BF), before, preferred_element_type=F32)
    rank_r = jnp.where(member_r, rank_r, -1.0)

    @pl.loop(0, TOK // 64)
    def _(i):
        r = pl.ds(pl.multiple_of(i * 64, 64), 64)
        v = tokens[r, :].astype(F32)
        scale = lax.rsqrt(jnp.mean(v * v, axis=-1, keepdims=True) + 1e-06)
        cols = pl.ds(pl.multiple_of(tp * WCOL, WCOL), WCOL)
        rr[r, :] = (tokens[r, cols].astype(F32) * scale).astype(BF)

    mine = rr[0:TOK, :]
    slot = lax.broadcasted_iota(jnp.int32, (NL, CAP, TOK), 1).astype(F32)
    for yy in range(NY):
        rk = rank_r[yy * NL : (yy + 1) * NL, :]
        pick = jnp.broadcast_to(rk[:, None, :], (NL, CAP, TOK)) == slot
        pick = pick.astype(F32).reshape(NL * CAP, TOK).astype(BF)
        got = jnp.dot(pick, mine, preferred_element_type=F32).reshape(NL, CAP, WCOL)
        ts[yy] = halves_down(got).astype(BF)

    g = jnp.broadcast_to(gain[...], (32, 128))[None, None]
    for yy in range(NY):
        for zt in range(NL):
            e = zt * NY + yy
            ws[yy, zt, :, 0:128] = (gate[e] * g[0, 0]).astype(BF)
            ws[yy, zt, :, 128:256] = (up[e] * g[0, 0]).astype(BF)
            ds[yy, zt] = down[e].astype(BF)

    pl.semaphore_wait(bar, (NY - 1) + (NZ - 1) + (NTP - 1))

    T, W, D = 0, 1, 2
    stage_y = ((ts, yt, T), (ws, yw, W), (ds, yd, D))

    def y_copy(kind, d):
        src, dst, k = stage_y[kind]
        to = (my + d) % NY
        return copy_to(src.at[to], dst.at[my], y_send.at[k, d], y_recv.at[k, d], {"y": to})

    for kind in (T, W, D):
        for d in (1, 3, 2):
            y_copy(kind, d).start()

    def tok_dist(delta):
        if delta < 4:
            return delta
        if delta > 4:
            return delta - NL
        return 4 - NL * (zl % 2)

    def z_tok(src, ys):
        for delta in (4, 3, 5, 2, 6, 1, 7):
            zt = (zl + delta) % NL
            copy_to(
                src.at[zt], xa.at[mx, mc, zl, ys], z_send.at[T], z_recv.at[T], at_z(zz + tok_dist(delta))
            ).start()
        pltpu.make_async_copy(src.at[zl], xa.at[mx, mc, zl, ys], loc.at[T]).start()

    def z_weights(src, into, k, ys):
        def send(far):
            copy_to(src.at[far % NL], into.at[zz, ys], z_send.at[k], z_recv.at[k], at_z(far)).start()

        send(zz + NL)

        @pl.loop(1, NL)
        def _(i):
            send(zz + NL + i)
            send(zz + NL - i)

        pltpu.make_async_copy(src.at[zl], into.at[zz, ys], loc.at[k]).start()

    z_tok(ts.at[my], my)
    z_weights(ws.at[my], gw, W, my)
    for d in (1, 3, 2):
        y_copy(T, d).wait_recv()
        ys = (my + NY - d) % NY
        z_tok(yt.at[ys], ys)
    for d in (1, 3, 2):
        y_copy(W, d).wait_recv()
        ys = (my + NY - d) % NY
        z_weights(yw.at[ys], gw, W, ys)
    z_weights(ds.at[my], dw, D, my)
    for d in (1, 3, 2):
        y_copy(D, d).wait_recv()
        ys = (my + NY - d) % NY
        z_weights(yd.at[ys], dw, D, ys)

    first_c, second_c = relabel(idsc[:, 0:1]), relabel(idsc[:, 1:2])
    exc = lax.broadcasted_iota(jnp.int32, (TOK, EXP), 1)
    is_first, is_second = exc == first_c, exc == second_c
    after = (a > b).astype(F32).astype(BF)
    rank_c = jnp.dot(after, (is_first | is_second).astype(F32).astype(BF), preferred_element_type=F32)
    place = lax.broadcasted_iota(jnp.int32, (TOK, ROWS), 1).astype(F32)
    for is_k, e_k, q in ((is_first, first_c, q0), (is_second, second_c, q1)):
        at = jnp.sum(jnp.where(is_k, rank_c, 0.0), axis=1, keepdims=True) + e_k.astype(F32) * CAP
        q[...] = (place == at).astype(F32).astype(BF)

    wait_bytes(xa.at[0, 0, 0], loc.at[T])
    wait_bytes(xa.at[0, 0, 0:7], z_recv.at[T])

    def x_copy(ref, k, d):
        to = (mx + d) % NX
        return copy_to(ref.at[mx, mc], ref.at[mx, mc], x_send.at[k, d], x_recv.at[k, d], {"x": to})

    def c_copy(ref, k, d):
        who = (mx + NX - d) % NX
        return copy_to(
            ref.at[who, mc], ref.at[who, mc], x_send.at[k, NX + d], x_recv.at[k, NX + d], {"c": 1 - mc}
        )

    def gather_tp(ref, k):
        for d in (1, 3, 2):
            x_copy(ref, k, d).start()
        c_copy(ref, k, 0).start()
        for d in (1, 3, 2):
            x_copy(ref, k, d).wait_recv()
            c_copy(ref, k, d).start()
        for d in range(NX):
            c_copy(ref, k, d).wait_recv()

    gather_tp(xa, 0)

    @pl.loop(0, NL)
    def _(i):
        r = pl.ds(pl.multiple_of(i * NY * CAP, NY * CAP), NY * CAP)
        for x in range(NX):
            for c in range(NC):
                v = xa[x, c, i].astype(F32)
                col = (x * NC + c) * WCOL
                xr[r, col : col + 128] = v[:, :CAP].reshape(NY * CAP, 128).astype(BF)
                xr[r, col + 128 : col + 256] = v[:, CAP:].reshape(NY * CAP, 128).astype(BF)

    wait_bytes(gw.at[0], loc.at[W])
    wait_bytes(gw.at[0:15], z_recv.at[W])
    gate_copy = pltpu.make_async_copy(gw.at[:, :, :, 0:128], gate_out, out_sem.at[0])
    up_copy = pltpu.make_async_copy(gw.at[:, :, :, 128:256], up_out, out_sem.at[1])
    gate_copy.start()
    up_copy.start()
    hid_rows = 128

    @pl.loop(0, ROWS // hid_rows)
    def _(i):
        r = pl.ds(pl.multiple_of(i * hid_rows, hid_rows), hid_rows)
        both = jnp.dot(xr[r, :], gw[...].reshape(WIDTH, 256), preferred_element_type=F32)
        v = both[:, 0:128]
        hh[mx, mc, r, :] = (v / (1.0 + jnp.exp(-v)) * both[:, 128:256]).astype(BF)

    gather_tp(hh, 1)

    wait_bytes(dw.at[0], loc.at[D])
    wait_bytes(dw.at[0:15], z_recv.at[D])

    def tp_copy(d):
        t = (tp + d) % NTP
        return copy_to(
            dw.at[pl.ds(t * 2, 2)], dn.at[tp], x_send.at[2, d], x_recv.at[2, d], {"x": t // NC, "c": t % NC}
        )

    own_dn = pltpu.make_async_copy(dw.at[pl.ds(tp * 2, 2)], dn.at[tp], loc.at[3])

    def back_dist(delta):
        if delta < 4:
            return -delta
        if delta > 4:
            return NL - delta
        return NL * (zl % 2) - 4

    order = (4, 3, 5, 2, 6, 1, 7, 0)

    def back_z(delta):
        src_zl = (zl + NL - delta) % NL
        return copy_to(
            os_.at[src_zl], rz.at[zl], b_send.at[delta], b_recv.at[delta], at_z(zz + back_dist(delta))
        )

    def back_y(delta):
        ex_zl = (zl + delta) % NL
        src = rz.at[ex_zl] if delta else os_.at[zl]
        for d in (2, 1, 3):
            to = (my + d) % NY
            copy_to(src.at[to], rt.at[my, ex_zl], c_sem.at[0], c_sem.at[1], {"y": to}).start()
        pltpu.make_async_copy(src.at[my], rt.at[my, ex_zl], c_sem.at[2]).start()

    for delta in order:
        src_zl = (zl + NL - delta) % NL
        r = pl.ds(pl.multiple_of(src_zl * NY * CAP, NY * CAP), NY * CAP)
        acc = jnp.zeros((NY * CAP, WCOL), F32)
        for x in range(NX):
            lhs = jnp.concatenate([hh[x, 0, r, :], hh[x, 1, r, :]], axis=1)
            acc += jnp.dot(lhs, dw[4 * x : 4 * x + 4].reshape(256, WCOL), preferred_element_type=F32)
        os_[src_zl] = halves_down(acc.reshape(NY, CAP, WCOL)).astype(BF)
        if delta:
            back_z(delta).start()
    back_y(0)
    own_dn.start()
    for d in (1, 7, 2, 6, 3, 5, 4):
        tp_copy(d).start()
    for delta in (1, 7, 2, 6, 3, 5, 4):
        back_z(delta).wait_recv()
        back_y(delta)

    own_dn.wait()
    for d in range(1, NTP):
        tp_copy(d).wait_recv()
    dn_copies = [
        pltpu.make_async_copy(
            dn.at[t].reshape(128, WCOL), down_out.at[:, t * WCOL : (t + 1) * WCOL], out_sem.at[2 + t]
        )
        for t in range(NTP)
    ]
    for copy in dn_copies:
        copy.start()

    wait_bytes(rt.at[0], c_sem.at[2])
    wait_bytes(rt.at[0:3], c_sem.at[1])
    for yy in range(NY):
        v = rt[yy].astype(F32)
        r = slice(yy * NL * CAP, (yy + 1) * NL * CAP)
        rr[r, 0:128] = v[:, :CAP].reshape(NL * CAP, 128).astype(BF)
        rr[r, 128:256] = v[:, CAP:].reshape(NL * CAP, 128).astype(BF)

    for i in range(TOK // 128):
        r = slice(i * 128, (i + 1) * 128)
        one = jnp.dot(q0[r, :], rr[...], preferred_element_type=F32)
        two = jnp.dot(q1[r, :], rr[...], preferred_element_type=F32)
        mixed[r, :] = (wts[r, 0:1] * one + wts[r, 1:2] * two).astype(BF)

    gate_copy.wait()
    up_copy.wait()
    for copy in dn_copies:
        copy.wait()
    for kind in (T, W, D):
        for d in (1, 3, 2):
            y_copy(kind, d).wait_send()
    wait_bytes(xa.at[0, 0, 0:7], z_send.at[T])
    wait_bytes(gw.at[0:15], z_send.at[W])
    wait_bytes(dw.at[0:15], z_send.at[D])
    for ref, k in ((xa, 0), (hh, 1)):
        for d in (1, 3, 2):
            x_copy(ref, k, d).wait_send()
        for d in range(NX):
            c_copy(ref, k, d).wait_send()
    for d in range(1, NTP):
        tp_copy(d).wait_send()
    for delta in range(1, NL):
        back_z(delta).wait_send()
    wait_bytes(rt.at[0:3], c_sem.at[0])


def local(tokens, route_ids, route_weights, norm_gain, gate_weight, up_weight, down_weight):
    vm = pl.BlockSpec(memory_space=pltpu.VMEM)
    far = pl.BlockSpec(memory_space=pl.ANY)
    dma = pltpu.SemaphoreType.DMA
    gate_new, up_new, down_new, mixed = pl.pallas_call(
        kernel,
        out_shape=(
            jax.ShapeDtypeStruct((NZ, NY, 32, 128), BF),
            jax.ShapeDtypeStruct((NZ, NY, 32, 128), BF),
            jax.ShapeDtypeStruct((128, WIDTH), BF),
            jax.ShapeDtypeStruct((TOK, WCOL), BF),
        ),
        in_specs=[vm] * 8,
        out_specs=(far, far, far, vm),
        scratch_shapes=[
            pltpu.VMEM((NY, NL, 32, 256), BF),
            pltpu.VMEM((NY, NL, 32, 256), BF),
            pltpu.VMEM((NZ, NY, 32, 256), BF),
            pltpu.VMEM((NY, NL, 16, WCOL), BF),
            pltpu.VMEM((NY, NL, 16, WCOL), BF),
            pltpu.VMEM((NZ, NY, 16, WCOL), BF),
            pltpu.VMEM((NTP, 2, NY, 16, WCOL), BF),
            pltpu.VMEM((NY, NL, 2 * CAP, 128), BF),
            pltpu.VMEM((NY, NL, 2 * CAP, 128), BF),
            pltpu.VMEM((NX, NC, NL, NY, 2 * CAP, 128), BF),
            pltpu.VMEM((ROWS, WIDTH), BF),
            pltpu.VMEM((NX, NC, ROWS, 128), BF),
            pltpu.VMEM((NL, NY, 2 * CAP, 128), BF),
            pltpu.VMEM((NL, NY, 2 * CAP, 128), BF),
            pltpu.VMEM((NY, NL, 2 * CAP, 128), BF),
            pltpu.VMEM((ROWS, WCOL), BF),
            pltpu.VMEM((TOK, ROWS), BF),
            pltpu.VMEM((TOK, ROWS), BF),
            dma((3, NY)),
            dma((3, NY)),
            dma((3,)),
            dma((3,)),
            dma((3, NTP)),
            dma((3, NTP)),
            dma((NL,)),
            dma((NL,)),
            dma((3,)),
            dma((4,)),
            dma((2 + NTP,)),
        ],
        compiler_params=pltpu.CompilerParams(
            collective_id=0, has_side_effects=True, vmem_limit_bytes=56 * 1024 * 1024
        ),
        name="handoff",
    )(
        tokens,
        route_ids,
        route_ids.T,
        route_weights,
        norm_gain.reshape(32, 1),
        gate_weight,
        up_weight,
        down_weight,
    )
    return (
        gate_new.reshape(1, WIDTH, 128),
        up_new.reshape(1, WIDTH, 128),
        down_new.reshape(1, 128, WIDTH),
        mixed,
    )


def solution(mesh):
    torus = Mesh(mesh.devices.reshape(NH, NL, NY, NX, NC), ("zh", "zl", "y", "x", "c"))
    rows, cols = ("zh", "zl", "y"), ("x", "c")
    placed = (P(rows, None),) * 3 + (P(rows),) + (P(None, rows, cols),) * 3
    experts = ("zl", "y")
    return jax.shard_map(
        local,
        mesh=torus,
        in_specs=placed,
        out_specs=(P(experts, None, cols), P(experts, None, cols), P(experts, cols, None), P(rows, cols)),
        check_vma=False,
    )
```

time: 371 us -> 124 us (0.33)
  waiting for transfers between devices: 220 us -> 0 us
  Pallas kernels: 0 us -> 113 us
  blocking collectives: 62.1 us -> 0 us
  starting transfers between devices: 38.9 us -> 0 us
  between operations: 14.3 us -> 0.66 us
  other arithmetic: 8.64 us -> 0 us
  local copies, waits for them, and re-layouts: 16.8 us -> 9.63 us
  matrix products: 6.93 us -> 0 us
    all_to_all x4 -> x0, waiting for transfers between devices: 153 us -> none  [the longest x1 113 us: local(): lax.all_to_all(outgoing, 'fs', split_axis=0, concat_axis=0, tiled=True)]
    pallas_call x0 -> x1, Pallas kernels: none -> 113 us  [local(): pl.pallas_call(kernel, out_shape=(jax.ShapeDtypeStruct((NZ, NY, 32, 128),...]
    all_gather x2 -> x0, waiting for transfers between devices: 67.4 us -> none  [the longest x1 67.4 us: in_one_piece(): lax.all_gather(both, axis, axis=dim, tiled=True)]
    all_to_all x4 -> x0, starting transfers between devices: 38.8 us -> none  [the longest x1 16.2 us: side_by_side(): lax.all_to_all(both, axis, split_axis=split_dim, concat_axis=concat_dim,...]
    all_to_all x2 -> x0, blocking collectives: 38.3 us -> none  [the longest x1 25.1 us: local(): lax.all_to_all(down_rounded, 'fs', split_axis=0, concat_axis=1, tiled=True)]
    all_gather x1 -> x0, blocking collectives: 23.8 us -> none  [local(): lax.all_gather(moved[2], 'gr', axis=1, tiled=True)]
    unnamed x10, local copies, waits for them, and re-layouts: 0.29 us -> 8.29 us
    dot_general x3 -> x0, matrix products: 6.93 us -> none  [the longest x1 3.2 us: local(): jnp.einsum('mbf,bfd->bmd', piece.reshape(row_count, blocks, hidden_width)...]
  transfers between devices with their start and end apart: 6 -> 0, of which waited for: 5 -> 0; matrix products, arithmetic and copies ran while one was open for 6% -> 0% of each run, Pallas kernels for 0% -> 0%
where the time goes in v1:
time: 124 us; the launch traced here: 123 us
  Pallas kernels  113 us (91%)
  local copies, waits for them, and re-layouts  9.63 us (8%)
    pallas_call x1, Pallas kernels, local(): pl.pallas_call(kernel, out_shape=(jax.ShapeDtypeStruct((NZ, NY, 32, 128),...  113 us
    unnamed x10, local copies, waits for them, and re-layouts  8.29 us

profile of v1, /device:TPU:1, one launch (start us, length us, event | category | flops | bytes accessed | tf_op | source)
XLA Modules:
  0.0 123.4 jit_solution(6906460260671283133)
XLA Ops:
  0.6 1.3 %copy.13.gain = f32[32,1]{1,0:T(8,128)} copy(f32[32,1]{0,1:T(1,128)} %bitcast.9) | data formatting | bytes 256 | tf_op jit(solution)/shard_map/reshape | solution.py:371
  2.0 1.5 %copy.12.wts = f32[384,2]{1,0:T(8,128)} copy(f32[384,2]{0,1:T(2,128)} %param.9) | data formatting | bytes 6144 | tf_op args[2]
  3.5 1.5 %copy.11.idsc = s32[384,2]{1,0:T(8,128)} copy(s32[384,2]{0,1:T(2,128)} %param.8) | data formatting | bytes 6144 | tf_op args[1]
  5.0 113.1 %handoff.1 = (bf16[16,4,32,128]{3,2,1,0:T(8,128)(2,1)}, bf16[16,4,32,128]{3,2,1,0:T(8,128)(2,1)}, bf16[128,2048]{1,0:T(8,128)(2,1)}, bf16[384,256]{1,0:T(8,128)(2,1)}) custom-call(bf16[384,2048]{1,0:T(8,128)(2,1)} %tokens.1, s32[384,2]{1,0:T(8,128)} %copy.11.idsc, s32[2,384]{1,0:T(2,128)} %bitcast.8, f32[384,2]{1,0:T(8,128)} %copy.12.wts, ...), custom_call_target="tpu_custom_call" | custom-call | tf_op jit(solution)/shard_map/handoff/pallas_call | solution.py:321
  118.1 0.0 copy-start
  118.1 0.0 copy-start.1
  118.1 1.9 %copy.18 = bf16[1,2048,128]{2,1,0:T(8,128)(2,1)} copy(bf16[1,2048,128]{2,1,0:T(8,128)(2,1)} %bitcast.7) | data formatting | bytes 1048576
  120.0 1.9 %copy.19 = bf16[1,2048,128]{2,1,0:T(8,128)(2,1)} copy(bf16[1,2048,128]{2,1,0:T(8,128)(2,1)} %bitcast.6) | data formatting | bytes 1048576
  121.9 0.0 copy-done
  121.9 0.8 copy.20
  122.7 0.0 copy-done.1
  122.7 0.7 copy.21
Async XLA Ops:
  118.1 3.8 %copy-start = (bf16[128,2048]{1,0:T(8,128)(2,1)S(1)}, bf16[128,2048]{1,0:T(8,128)(2,1)}, u32[]{:S(2)}) copy-start(bf16[128,2048]{1,0:T(8,128)(2,1)} %get-tuple-element.10) | copy-start | bytes 1572868
  118.1 4.6 %copy-start.1 = (bf16[384,256]{1,0:T(8,128)(2,1)S(1)}, bf16[384,256]{1,0:T(8,128)(2,1)}, u32[]{:S(2)}) copy-start(bf16[384,256]{1,0:T(8,128)(2,1)} %get-tuple-element.19) | copy-start | bytes 589828

commit v2 on v1

v2 whole, which is shorter than its diff:
```python
import jax
import jax.numpy as jnp
from jax import lax
from jax.experimental import pallas as pl
from jax.experimental.pallas import tpu as pltpu
from jax.sharding import Mesh
from jax.sharding import PartitionSpec as P

MESH = pl.DeviceIdType.MESH
BF, F32 = jnp.bfloat16, jnp.float32
NZ, NH, NL, NY, NX, NC = 16, 2, 8, 4, 4, 2
NTP = NX * NC
TOK, WIDTH, CAP, EXP = 384, 2048, 24, 32
WCOL = WIDTH // NTP
ROWS = EXP * CAP
VMEM_MOVE, VMEM_LAST = 57, 57


def halves_down(v):
    return jnp.concatenate([v[:, :, :128], v[:, :, 128:]], axis=1)


def kernel(
    tokens_in, ids_in, wts_in, gain_in, gate_in, up_in, down_in,
    gw_out, dn, rt, cols_out,
    tokens, ids, wts, gain, gate, up, down, ws, yw, gw, ds, yd, dw, ts, yt, xa, xr, hh, os_, rr, cols,
    y_send, y_recv, z_send, z_recv, x_send, x_recv, b_send, b_recv, loc, in_sem, out_sem,
):
    zh, zl, my = lax.axis_index("zh"), lax.axis_index("zl"), lax.axis_index("y")
    mx, mc = lax.axis_index("x"), lax.axis_index("c")
    zz = zh * NL + zl
    tp = mx * NC + mc

    def at_z(z):
        z = (z + 2 * NZ) % NZ
        return {"zh": z // NL, "zl": z % NL}

    def copy_to(src, dst, send, recv, dev):
        return pltpu.make_async_remote_copy(
            src_ref=src, dst_ref=dst, send_sem=send, recv_sem=recv, device_id=dev, device_id_type=MESH
        )

    def wait_bytes(ref, sem):
        pltpu.make_async_copy(ref, ref, sem).wait()

    bar = pltpu.get_barrier_semaphore()

    def greet(dev):
        pl.semaphore_signal(bar, inc=1, device_id=dev, device_id_type=MESH)

    greet(at_z(zz + NL))

    @pl.loop(1, NL)
    def _(d):
        greet(at_z(zz + NL + d))
        greet(at_z(zz + NL - d))

    ins = [
        pltpu.make_async_copy(far, near, in_sem.at[i])
        for i, (far, near) in enumerate(
            (
                (gate_in, gate), (up_in, up), (gain_in, gain), (tokens_in, tokens), (ids_in, ids), (wts_in, wts),
                (down_in, down),
            )
        )
    ]
    for copy in ins:
        copy.start()

    @pl.loop(1, NY)
    def _(d):
        greet({"y": (my + d) % NY})

    @pl.loop(1, NTP)
    def _(d):
        t = (tp + d) % NTP
        greet({"x": t // NC, "c": t % NC})

    with jax.named_scope("w_gain"):
        ins[2].wait()
        eye = lax.broadcasted_iota(jnp.int32, (32, 32), 0) == lax.broadcasted_iota(jnp.int32, (32, 32), 1)
    g = jnp.sum(jnp.where(eye, jnp.broadcast_to(gain[...], (32, 32)), 0.0), axis=1, keepdims=True)
    g = jnp.broadcast_to(g, (32, 128))
    with jax.named_scope("fold"):
        ins[0].wait()
        ins[1].wait()
        for yy in range(NY):
            for zt in range(NL):
                e = zt * NY + yy
                ws[yy, zt, :, 0:128] = (gate[e] * g).astype(BF)
                ws[yy, zt, :, 128:256] = (up[e] * g).astype(BF)

    with jax.named_scope("w_bar"):
        pl.semaphore_wait(bar, (NY - 1) + (NZ - 1) + (NTP - 1))

    T, W, D = 0, 1, 2

    def y_copy(k, d):
        to = (my + d) % NY
        src, dst = (
            (ts.at[to], yt.at[my]) if k == T else (ws.at[to], yw.at[my]) if k == W else (ds.at[:, to], yd.at[:, my])
        )
        return copy_to(src, dst, y_send.at[k, d], y_recv.at[k, d], {"y": to})

    def tok_dist(delta):
        if delta < 4:
            return delta
        if delta > 4:
            return delta - NL
        return 4 - NL * (zl % 2)

    def z_tok(src, ys):
        for delta in (4, 3, 5, 2, 6, 1, 7):
            zt = (zl + delta) % NL
            copy_to(
                src.at[zt], xa.at[mx, mc, zl, ys], z_send.at[T], z_recv.at[T], at_z(zz + tok_dist(delta))
            ).start()
        pltpu.make_async_copy(src.at[zl], xa.at[mx, mc, zl, ys], loc.at[T]).start()

    def z_weights(src, into, k, ys):
        def send(far):
            copy_to(src.at[far % NL], into.at[zz, ys], z_send.at[k], z_recv.at[k], at_z(far)).start()

        send(zz + NL)

        @pl.loop(1, NL)
        def _(i):
            send(zz + NL + i)
            send(zz + NL - i)

        pltpu.make_async_copy(src.at[zl], into.at[zz, ys], loc.at[k]).start()

    def z_down(h):
        def send(far):
            copy_to(yd.at[h, :, far % NL], dw.at[h, zz], z_send.at[D + h], z_recv.at[D + h], at_z(far)).start()

        send(zz + NL)
        pltpu.make_async_copy(yd.at[h, :, zl], dw.at[h, zz], loc.at[D + h]).start()

        @pl.loop(1, NL)
        def _(i):
            send(zz + NL + i)
            send(zz + NL - i)

    with jax.named_scope("send_w"):
        for d in (1, 3, 2):
            y_copy(W, d).start()
        z_weights(ws.at[my], gw, W, my)

    def relabel(e):
        return (e % NY) * NL + e // NY

    ins[4].wait()
    ins[5].wait()
    first_r, second_r = relabel(ids[0:1, :]), relabel(ids[1:2, :])
    ex = lax.broadcasted_iota(jnp.int32, (EXP, TOK), 0)
    member_r = (ex == first_r) | (ex == second_r)
    a = lax.broadcasted_iota(jnp.int32, (TOK, TOK), 0)
    b = lax.broadcasted_iota(jnp.int32, (TOK, TOK), 1)
    before = (a < b).astype(F32).astype(BF)
    rank_r = jnp.dot(member_r.astype(F32).astype(BF), before, preferred_element_type=F32)
    rank_r = jnp.where(member_r, rank_r, -1.0)

    ins[3].wait()

    @pl.loop(0, TOK // 64)
    def _(i):
        r = pl.ds(pl.multiple_of(i * 64, 64), 64)
        v = tokens[r, :].astype(F32)
        scale = lax.rsqrt(jnp.mean(v * v, axis=-1, keepdims=True) + 1e-06)
        own = pl.ds(pl.multiple_of(tp * WCOL, WCOL), WCOL)
        rr[r, :] = (tokens[r, own].astype(F32) * scale).astype(BF)

    mine = rr[0:TOK, :]
    slot = lax.broadcasted_iota(jnp.int32, (NL, CAP, TOK), 1).astype(F32)
    for yy in range(NY):
        rk = rank_r[yy * NL : (yy + 1) * NL, :]
        pick = jnp.broadcast_to(rk[:, None, :], (NL, CAP, TOK)) == slot
        pick = pick.astype(F32).reshape(NL * CAP, TOK).astype(BF)
        got = jnp.dot(pick, mine, preferred_element_type=F32).reshape(NL, CAP, WCOL)
        ts[yy] = halves_down(got).astype(BF)

    with jax.named_scope("send_t"):
        for d in (1, 3, 2):
            y_copy(T, d).start()
        z_tok(ts.at[my], my)

    ins[6].wait()
    for yy in range(NY):
        for zt in range(NL):
            both = down[zt * NY + yy].astype(BF)
            ds[0, yy, zt] = both[:, 0:128]
            ds[1, yy, zt] = both[:, 128:256]

    for d in (1, 3, 2):
        y_copy(D, d).start()
    own_down = pltpu.make_async_copy(ds.at[:, my], yd.at[:, my], loc.at[4])
    own_down.start()
    with jax.named_scope("fwd_t"):
        for d in (1, 3, 2):
            y_copy(T, d).wait_recv()
            ys = (my + NY - d) % NY
            z_tok(yt.at[ys], ys)
    with jax.named_scope("fwd_w"):
        for d in (1, 3, 2):
            y_copy(W, d).wait_recv()
            ys = (my + NY - d) % NY
            z_weights(yw.at[ys], gw, W, ys)
    with jax.named_scope("fwd_d"):
        for d in (1, 3, 2):
            y_copy(D, d).wait_recv()
        own_down.wait()
        z_down(0)
        z_down(1)

    ats = [
        jnp.sum(jnp.where(ex == e_k, rank_r, 0.0), axis=0, keepdims=True) + e_k.astype(F32) * CAP
        for e_k in (first_r, second_r)
    ]
    turned = jnp.concatenate([*ats, wts[...], jnp.zeros((4, TOK), F32)], axis=0).T
    cols[...] = jnp.concatenate([turned, jnp.zeros((TOK, 120), F32)], axis=1)
    outs = [
        pltpu.make_async_copy(near, far, out_sem.at[i])
        for i, (near, far) in enumerate(((cols, cols_out), (gw, gw_out)))
    ]
    outs[0].start()

    with jax.named_scope("w_ztok"):
        wait_bytes(xa.at[0, 0, 0], loc.at[T])
        wait_bytes(xa.at[0, 0, 0:7], z_recv.at[T])

    def x_copy(ref, k, d):
        to = (mx + d) % NX
        return copy_to(ref.at[mx, mc], ref.at[mx, mc], x_send.at[k, d], x_recv.at[k, d], {"x": to})

    def c_copy(ref, k, d):
        who = (mx + NX - d) % NX
        return copy_to(
            ref.at[who, mc], ref.at[who, mc], x_send.at[k, NX + d], x_recv.at[k, NX + d], {"c": 1 - mc}
        )

    def gather_tp(ref, k):
        for d in (1, 3, 2):
            x_copy(ref, k, d).start()
        c_copy(ref, k, 0).start()
        for d in (1, 3, 2):
            x_copy(ref, k, d).wait_recv()
            c_copy(ref, k, d).start()
        for d in range(NX):
            c_copy(ref, k, d).wait_recv()

    with jax.named_scope("gather_x"):
        gather_tp(xa, 0)

    @pl.loop(0, NL)
    def _(i):
        r = pl.ds(pl.multiple_of(i * NY * CAP, NY * CAP), NY * CAP)
        for x in range(NX):
            for c in range(NC):
                v = xa[x, c, i].astype(F32)
                col = (x * NC + c) * WCOL
                xr[r, col : col + 128] = v[:, :CAP].reshape(NY * CAP, 128).astype(BF)
                xr[r, col + 128 : col + 256] = v[:, CAP:].reshape(NY * CAP, 128).astype(BF)

    with jax.named_scope("w_zw"):
        wait_bytes(gw.at[0], loc.at[W])
        wait_bytes(gw.at[0:15], z_recv.at[W])
    outs[1].start()
    hid_rows = 128

    @pl.loop(0, ROWS // hid_rows)
    def _(i):
        r = pl.ds(pl.multiple_of(i * hid_rows, hid_rows), hid_rows)
        both = jnp.dot(xr[r, :], gw[...].reshape(WIDTH, 256), preferred_element_type=F32)
        v = both[:, 0:128]
        hh[mx, mc, r, :] = (v / (1.0 + jnp.exp(-v)) * both[:, 128:256]).astype(BF)

    with jax.named_scope("gather_h"):
        gather_tp(hh, 1)

    def back_dist(delta):
        if delta < 4:
            return -delta
        if delta > 4:
            return NL - delta
        return NL * (zl % 2) - 4


    def tp_copy(h, d):
        t = (tp + d) % NTP
        return copy_to(
            dw.at[h, pl.ds(t * 2, 2)], dn.at[tp, h], x_send.at[2 + h, d], x_recv.at[2 + h, d],
            {"x": t // NC, "c": t % NC},
        )

    def own_dn(h):
        return pltpu.make_async_copy(dw.at[h, pl.ds(tp * 2, 2)], dn.at[tp, h], loc.at[5 + h])

    def back(h, delta, ys):
        return copy_to(
            os_.at[h, (zl + NL - delta) % NL, ys], rt.at[h, my, zl], b_send.at[h, min(delta, 1)], b_recv.at[h],
            {**at_z(zz + back_dist(delta)), "y": ys},
        )

    def back_own(h):
        return pltpu.make_async_copy(os_.at[h, zl, my], rt.at[h, my, zl], b_recv.at[h])

    def give_back(h):
        with jax.named_scope("w_zd"):
            wait_bytes(dw.at[h, 0], loc.at[D + h])
            wait_bytes(dw.at[h, 0:15], z_recv.at[D + h])
        for delta in (4, 3, 5, 2, 6, 1, 7, 0):
            src_zl = (zl + NL - delta) % NL
            r = pl.ds(pl.multiple_of(src_zl * NY * CAP, NY * CAP), NY * CAP)
            acc = jnp.zeros((NY * CAP, 128), F32)
            for x in range(NX):
                lhs = jnp.concatenate([hh[x, 0, r, :], hh[x, 1, r, :]], axis=1)
                acc += jnp.dot(lhs, dw[h, 4 * x : 4 * x + 4].reshape(256, 128), preferred_element_type=F32)
            os_[h, src_zl] = acc.reshape(NY, 3, 8, 128).astype(BF)
            for d in range(NY):
                if delta or d:
                    back(h, delta, (my + d) % NY).start()
        back_own(h).start()
        own_dn(h).start()
        for d in (1, 7, 2, 6, 3, 5, 4):
            tp_copy(h, d).start()

    with jax.named_scope("give0"):
        give_back(0)
    with jax.named_scope("give1"):
        give_back(1)
    with jax.named_scope("w_back"):
        for h in range(2):
            wait_bytes(rt.at[h], b_recv.at[h])

    with jax.named_scope("drain"):
        for h in range(2):
            own_dn(h).wait()
            for d in range(1, NTP):
                tp_copy(h, d).wait()
            wait_bytes(dw.at[h, 0:15], z_send.at[D + h])
            wait_bytes(os_.at[h, 0, 0:3], b_send.at[h, 0])
            wait_bytes(os_.at[h, 0:7], b_send.at[h, 1])
        for copy in outs:
            copy.wait()
        for kind in (T, W, D):
            for d in (1, 3, 2):
                y_copy(kind, d).wait_send()
        wait_bytes(xa.at[0, 0, 0:7], z_send.at[T])
        wait_bytes(gw.at[0:15], z_send.at[W])
        for ref, k in ((xa, 0), (hh, 1)):
            for d in (1, 3, 2):
                x_copy(ref, k, d).wait_send()
            for d in range(NX):
                c_copy(ref, k, d).wait_send()


def finish(
    gw_in, dn_in, rt_in, cols_in, gate_out, up_out, down_out, mixed_out, gw, dn, rt, cols, rr, mixed, in_sem, sem
):
    ins = [
        pltpu.make_async_copy(far, near, in_sem.at[i])
        for i, (far, near) in enumerate(((cols_in, cols), (rt_in, rt), (gw_in, gw), (dn_in, dn)))
    ]
    for copy in ins:
        copy.start()
    place = lax.broadcasted_iota(jnp.int32, (TOK, ROWS), 1).astype(F32)
    ins[0].wait()
    q0 = (place == cols[:, 0:1]).astype(F32).astype(BF)
    q1 = (place == cols[:, 1:2]).astype(F32).astype(BF)

    ins[1].wait()
    for h in range(2):
        for yy in range(NY):
            r = slice(yy * NL * CAP, (yy + 1) * NL * CAP)
            rr[r, h * 128 : h * 128 + 128] = rt[h, yy].astype(F32).reshape(NL * CAP, 128).astype(BF)
    copies = []

    def put(near, far):
        copies.append(pltpu.make_async_copy(near, far, sem.at[len(copies)]))
        copies[-1].start()

    ins[2].wait()
    put(gw.at[:, :, :, 0:128], gate_out)
    put(gw.at[:, :, :, 128:256], up_out)
    ins[3].wait()
    for t in range(NTP):
        for h in range(2):
            at = t * WCOL + h * 128
            put(dn.at[t, h], down_out.at[:, :, :, at : at + 128])
    for i in range(TOK // 128):
        r = slice(i * 128, (i + 1) * 128)
        one = jnp.dot(q0[r, :], rr[...], preferred_element_type=F32)
        two = jnp.dot(q1[r, :], rr[...], preferred_element_type=F32)
        mixed[r, :] = (cols[r, 2:3] * one + cols[r, 3:4] * two).astype(BF)
        put(mixed.at[r], mixed_out.at[r])
    for copy in copies:
        copy.wait()


def local(tokens, route_ids, route_weights, norm_gain, gate_weight, up_weight, down_weight):
    hbm = pl.BlockSpec(memory_space=pltpu.HBM)
    free = pl.BlockSpec(memory_space=pl.ANY)
    dma = pltpu.SemaphoreType.DMA
    moved = pl.pallas_call(
        kernel,
        out_shape=(
            jax.ShapeDtypeStruct((NZ, NY, 32, 256), BF),
            jax.ShapeDtypeStruct((NTP, 2, 2, NY, 16, 128), BF),
            jax.ShapeDtypeStruct((2, NY, NL, 3, 8, 128), BF),
            jax.ShapeDtypeStruct((TOK, 128), F32),
        ),
        in_specs=[hbm] * 7,
        out_specs=(free,) * 4,
        scratch_shapes=[
            pltpu.VMEM((TOK, WIDTH), BF),
            pltpu.VMEM((2, TOK), jnp.int32),
            pltpu.VMEM((2, TOK), F32),
            pltpu.VMEM((1, 32), F32),
            pltpu.VMEM((EXP, 32, 128), F32),
            pltpu.VMEM((EXP, 32, 128), F32),
            pltpu.VMEM((EXP, 16, WCOL), F32),
            pltpu.VMEM((NY, NL, 32, 256), BF),
            pltpu.VMEM((NY, NL, 32, 256), BF),
            pltpu.VMEM((NZ, NY, 32, 256), BF),
            pltpu.VMEM((2, NY, NL, 16, 128), BF),
            pltpu.VMEM((2, NY, NL, 16, 128), BF),
            pltpu.VMEM((2, NZ, NY, 16, 128), BF),
            pltpu.VMEM((NY, NL, 2 * CAP, 128), BF),
            pltpu.VMEM((NY, NL, 2 * CAP, 128), BF),
            pltpu.VMEM((NX, NC, NL, NY, 2 * CAP, 128), BF),
            pltpu.VMEM((ROWS, WIDTH), BF),
            pltpu.VMEM((NX, NC, ROWS, 128), BF),
            pltpu.VMEM((2, NL, NY, 3, 8, 128), BF),
            pltpu.VMEM((TOK, WCOL), BF),
            pltpu.VMEM((TOK, 128), F32),
            dma((3, NY)),
            dma((3, NY)),
            dma((4,)),
            dma((4,)),
            dma((4, NTP)),
            dma((4, NTP)),
            dma((2, 2)),
            dma((2,)),
            dma((7,)),
            dma((7,)),
            dma((2,)),
        ],
        compiler_params=pltpu.CompilerParams(
            collective_id=0, has_side_effects=True, vmem_limit_bytes=VMEM_MOVE * 1024 * 1024
        ),
        name="handoff",
    )(
        tokens,
        route_ids.T,
        route_weights.T,
        norm_gain.reshape(1, 32),
        gate_weight,
        up_weight,
        down_weight,
    )
    gate_new, up_new, down_new, mixed = pl.pallas_call(
        finish,
        out_shape=(
            jax.ShapeDtypeStruct((NZ, NY, 32, 128), BF),
            jax.ShapeDtypeStruct((NZ, NY, 32, 128), BF),
            jax.ShapeDtypeStruct((2, NY, 16, WIDTH), BF),
            jax.ShapeDtypeStruct((TOK, WCOL), BF),
        ),
        in_specs=[hbm] * 4,
        out_specs=(hbm,) * 4,
        scratch_shapes=[
            pltpu.VMEM((NZ, NY, 32, 256), BF),
            pltpu.VMEM((NTP, 2, 2, NY, 16, 128), BF),
            pltpu.VMEM((2, NY, NL, 3, 8, 128), BF),
            pltpu.VMEM((TOK, 128), F32),
            pltpu.VMEM((ROWS, WCOL), BF),
            pltpu.VMEM((TOK, WCOL), BF),
            dma((4,)),
            dma((2 + 2 * NTP + TOK // 128,)),
        ],
        compiler_params=pltpu.CompilerParams(vmem_limit_bytes=VMEM_LAST * 1024 * 1024),
        name="finish",
    )(*moved)
    return (
        gate_new.reshape(1, WIDTH, 128),
        up_new.reshape(1, WIDTH, 128),
        down_new.reshape(1, 128, WIDTH),
        mixed,
    )


def solution(mesh):
    torus = Mesh(mesh.devices.reshape(NH, NL, NY, NX, NC), ("zh", "zl", "y", "x", "c"))
    rows, cols = ("zh", "zl", "y"), ("x", "c")
    placed = (P(rows, None),) * 3 + (P(rows),) + (P(None, rows, cols),) * 3
    experts = ("zl", "y")
    return jax.shard_map(
        local,
        mesh=torus,
        in_specs=placed,
        out_specs=(P(experts, None, cols), P(experts, None, cols), P(experts, cols, None), P(rows, cols)),
        check_vma=False,
    )
```

time: 124 us -> 108 us (0.87)
  local copies, waits for them, and re-layouts: 9.63 us -> 0 us
  Pallas kernels: 113 us -> 106 us
    unnamed x10 -> x0, local copies, waits for them, and re-layouts: 8.29 us -> none
    pallas_call x1 -> x2, Pallas kernels: 113 us -> 106 us  [the longest x1 103 us: local(): pl.pallas_call(kernel, out_shape=(jax.ShapeDtypeStruct((NZ, NY, 32, 256),...]
    reshape x1 -> x0, local copies, waits for them, and re-layouts: 1.34 us -> none  [local(): norm_gain.reshape(32, 1)]
where the time goes in v2:
time: 108 us; the launch traced here: 107 us
  Pallas kernels  106 us (98%)
    pallas_call x1, Pallas kernels, local(): pl.pallas_call(kernel, out_shape=(jax.ShapeDtypeStruct((NZ, NY, 32, 256),...  103 us
    pallas_call x1, Pallas kernels, local(): pl.pallas_call(finish, out_shape=(jax.ShapeDtypeStruct((NZ, NY, 32, 128),...  2.92 us

profile of v2, /device:TPU:1, one launch (start us, length us, event | category | flops | bytes accessed | tf_op | source)
XLA Modules:
  0.0 107.1 jit_solution(13833141282950574994)
XLA Ops:
  0.6 103.5 %handoff.1 = (bf16[16,4,32,256]{3,2,1,0:T(8,128)(2,1)}, bf16[8,2,2,4,16,128]{5,4,3,2,1,0:T(8,128)(2,1)}, bf16[2,4,8,3,8,128]{5,4,3,2,1,0:T(8,128)(2,1)}, f32[384,128]{1,0:T(8,128)}) custom-call(bf16[384,2048]{1,0:T(8,128)(2,1)} %tokens_in.1, s32[2,384]{1,0:T(2,128)} %bitcast.6, f32[2,384]{1,0:T(2,128)} %bitcast.7, f32[1,32]{1,0:T(1,128)} %bitcast.8, ...), custom_call_target="tpu_custom_call" | custom-call | tf_op jit(solution)/shard_map/handoff/pallas_call | solution.py:405
  104.1 2.9 %finish.1 = (bf16[16,4,32,128]{3,2,1,0:T(8,128)(2,1)}, bf16[16,4,32,128]{3,2,1,0:T(8,128)(2,1)}, bf16[2,4,16,2048]{3,2,1,0:T(8,128)(2,1)}, bf16[384,256]{1,0:T(8,128)(2,1)}) custom-call(bf16[16,4,32,256]{3,2,1,0:T(8,128)(2,1)} %get-tuple-element.12.gw_in, bf16[8,2,2,4,16,128]{5,4,3,2,1,0:T(8,128)(2,1)} %get-tuple-element.13.dn_in, ...), custom_call_target="tpu_custom_call" | custom-call | tf_op jit(solution)/shard_map/finish/pallas_call | solution.py:462

commit v3 on v2

--- a/solution.py
+++ b/solution.py
@@ -13,6 +13,7 @@
 TOK, WIDTH, CAP, EXP = 384, 2048, 24, 32
 WCOL = WIDTH // NTP
 ROWS = EXP * CAP
+NEAR = 4
 VMEM_MOVE, VMEM_LAST = 57, 57
 
 
@@ -24,7 +25,7 @@
     tokens_in, ids_in, wts_in, gain_in, gate_in, up_in, down_in,
     gw_out, dn, rt, cols_out,
     tokens, ids, wts, gain, gate, up, down, ws, yw, gw, ds, yd, dw, ts, yt, xa, xr, hh, os_, rr, cols,
-    y_send, y_recv, z_send, z_recv, x_send, x_recv, b_send, b_recv, loc, in_sem, out_sem,
+    y_send, y_recv, z_send, z_recv, x_send, x_recv, b_send, b_recv, loc, in_sem, out_sem, far_in,
 ):
     zh, zl, my = lax.axis_index("zh"), lax.axis_index("zl"), lax.axis_index("y")
     mx, mc = lax.axis_index("x"), lax.axis_index("c")
@@ -48,12 +49,10 @@
     def greet(dev):
         pl.semaphore_signal(bar, inc=1, device_id=dev, device_id_type=MESH)
 
-    greet(at_z(zz + NL))
-
-    @pl.loop(1, NL)
-    def _(d):
-        greet(at_z(zz + NL + d))
-        greet(at_z(zz + NL - d))
+    @pl.loop(0, NEAR)
+    def _(i):
+        greet(at_z(zz + NEAR - i))
+        greet(at_z(zz + NZ - NEAR + i))
 
     ins = [
         pltpu.make_async_copy(far, near, in_sem.at[i])
@@ -91,7 +90,9 @@
                 ws[yy, zt, :, 128:256] = (up[e] * g).astype(BF)
 
     with jax.named_scope("w_bar"):
-        pl.semaphore_wait(bar, (NY - 1) + (NZ - 1) + (NTP - 1))
+        pl.semaphore_wait(bar, (NY - 1) + 2 * NEAR + (NTP - 1))
+    for i, z in enumerate((zz + NEAR, zz + NZ - NEAR)):
+        pl.semaphore_signal(far_in.at[i], inc=1, device_id=at_z(z), device_id_type=MESH)
 
     T, W, D = 0, 1, 2
 
@@ -142,10 +143,18 @@
             send(zz + NL + i)
             send(zz + NL - i)
 
+    def own_w(far):
+        copy_to(ws.at[my, far % NL], gw.at[zz, my], z_send.at[W], z_recv.at[W], at_z(far)).start()
+
     with jax.named_scope("send_w"):
         for d in (1, 3, 2):
             y_copy(W, d).start()
-        z_weights(ws.at[my], gw, W, my)
+        pltpu.make_async_copy(ws.at[my, zl], gw.at[zz, my], loc.at[W]).start()
+
+        @pl.loop(0, NEAR)
+        def _(i):
+            own_w(zz + NEAR - i)
+            own_w(zz + NZ - NEAR + i)
 
     def relabel(e):
         return (e % NY) * NL + e // NY
@@ -184,6 +193,16 @@
         for d in (1, 3, 2):
             y_copy(T, d).start()
         z_tok(ts.at[my], my)
+
+    with jax.named_scope("w_far"):
+        pl.semaphore_wait(far_in.at[0], 1)
+        pl.semaphore_wait(far_in.at[1], 1)
+        own_w(zz + NL)
+
+        @pl.loop(1, NL - NEAR)
+        def _(i):
+            own_w(zz + NL + i)
+            own_w(zz + NL - i)
 
     ins[6].wait()
     for yy in range(NY):
@@ -445,6 +464,7 @@
             dma((7,)),
             dma((7,)),
             dma((2,)),
+            pltpu.SemaphoreType.REGULAR((2,)),
         ],
         compiler_params=pltpu.CompilerParams(
             collective_id=0, has_side_effects=True, vmem_limit_bytes=VMEM_MOVE * 1024 * 1024

time: 108 us -> 106 us (0.981); the launches traced: 107 us -> 106 us
  no operation moved by 1% of the time
where the time goes in v3:
time: 106 us
  Pallas kernels  106 us (100%)
    pallas_call x1, Pallas kernels, local(): pl.pallas_call(kernel, out_shape=(jax.ShapeDtypeStruct((NZ, NY, 32, 256),...  103 us
    pallas_call x1, Pallas kernels, local(): pl.pallas_call(finish, out_shape=(jax.ShapeDtypeStruct((NZ, NY, 32, 128),...  2.92 us

profile of v3, /device:TPU:1, one launch (start us, length us, event | category | flops | bytes accessed | tf_op | source)
XLA Modules:
  0.0 106.2 jit_solution(17725356326881853580)
XLA Ops:
  0.6 102.6 %handoff.1 = (bf16[16,4,32,256]{3,2,1,0:T(8,128)(2,1)}, bf16[8,2,2,4,16,128]{5,4,3,2,1,0:T(8,128)(2,1)}, bf16[2,4,8,3,8,128]{5,4,3,2,1,0:T(8,128)(2,1)}, f32[384,128]{1,0:T(8,128)}) custom-call(bf16[384,2048]{1,0:T(8,128)(2,1)} %tokens_in.1, s32[2,384]{1,0:T(2,128)} %bitcast.6, f32[2,384]{1,0:T(2,128)} %bitcast.7, f32[1,32]{1,0:T(1,128)} %bitcast.8, ...), custom_call_target="tpu_custom_call" | custom-call | tf_op jit(solution)/shard_map/handoff/pallas_call | solution.py:424
  103.3 2.9 %finish.1 = (bf16[16,4,32,128]{3,2,1,0:T(8,128)(2,1)}, bf16[16,4,32,128]{3,2,1,0:T(8,128)(2,1)}, bf16[2,4,16,2048]{3,2,1,0:T(8,128)(2,1)}, bf16[384,256]{1,0:T(8,128)(2,1)}) custom-call(bf16[16,4,32,256]{3,2,1,0:T(8,128)(2,1)} %get-tuple-element.12.gw_in, bf16[8,2,2,4,16,128]{5,4,3,2,1,0:T(8,128)(2,1)} %get-tuple-element.13.dn_in, ...), custom_call_target="tpu_custom_call" | custom-call | tf_op jit(solution)/shard_map/finish/pallas_call | solution.py:482

commit v4 on v3

--- a/solution.py
+++ b/solution.py
@@ -13,7 +13,8 @@
 TOK, WIDTH, CAP, EXP = 384, 2048, 24, 32
 WCOL = WIDTH // NTP
 ROWS = EXP * CAP
-NEAR = 4
+NEAR, CUT = 4, 4
+NG, GT = 4, TOK // 4
 VMEM_MOVE, VMEM_LAST = 57, 57
 
 
@@ -24,8 +25,8 @@
 def kernel(
     tokens_in, ids_in, wts_in, gain_in, gate_in, up_in, down_in,
     gw_out, dn, rt, cols_out,
-    tokens, ids, wts, gain, gate, up, down, ws, yw, gw, ds, yd, dw, ts, yt, xa, xr, hh, os_, rr, cols,
-    y_send, y_recv, z_send, z_recv, x_send, x_recv, b_send, b_recv, loc, in_sem, out_sem, far_in,
+    tokens, ids, wts, gain, gate, up, down, ws, yw, gw, ds, yd, dw, gs, gb, yt, xa, xr, hh, os_, rr, cols,
+    y_send, y_recv, z_send, z_recv, x_send, x_recv, b_send, b_recv, loc, in_sem, out_sem, far_in, g_send, g_recv, t_send, t_recv, h_send, h_recv,
 ):
     zh, zl, my = lax.axis_index("zh"), lax.axis_index("zl"), lax.axis_index("y")
     mx, mc = lax.axis_index("x"), lax.axis_index("c")
@@ -99,24 +100,26 @@
     def y_copy(k, d):
         to = (my + d) % NY
         src, dst = (
-            (ts.at[to], yt.at[my]) if k == T else (ws.at[to], yw.at[my]) if k == W else (ds.at[:, to], yd.at[:, my])
+            (yt.at[to], xa.at[mx, mc, :, my]) if k == T else (ws.at[to], yw.at[my]) if k == W else (ds.at[:, to], yd.at[:, my])
         )
         return copy_to(src, dst, y_send.at[k, d], y_recv.at[k, d], {"y": to})
 
-    def tok_dist(delta):
-        if delta < 4:
-            return delta
-        if delta > 4:
-            return delta - NL
-        return 4 - NL * (zl % 2)
-
-    def z_tok(src, ys):
-        for delta in (4, 3, 5, 2, 6, 1, 7):
-            zt = (zl + delta) % NL
-            copy_to(
-                src.at[zt], xa.at[mx, mc, zl, ys], z_send.at[T], z_recv.at[T], at_z(zz + tok_dist(delta))
-            ).start()
-        pltpu.make_async_copy(src.at[zl], xa.at[mx, mc, zl, ys], loc.at[T]).start()
+    par = zl % 2
+    toward = 1 - 2 * par
+
+    def tok_src(i):
+        return (zl + NL - i * toward) % NL
+
+    def tok_send(i):
+        j = (0, 3 - 2 * par, 1 + 2 * par, 2)[i]
+        off = (0, 2 * par - 1, 2 - 4 * par, 6 * par - 3)[i]
+        return copy_to(gs.at[(zl // 2 + j) % NG], gb.at[zl], g_send.at[0, i], g_recv.at[0, i], at_z(zz + off))
+
+    def tok_relay(i):
+        src = gb.at[tok_src(i)] if i else gs.at[zl // 2]
+        return copy_to(src, gb.at[tok_src(i)], g_send.at[1, i], g_recv.at[1, i], at_z(zz + toward))
+
+    own_group = pltpu.make_async_copy(gs.at[zl // 2], gb.at[zl], loc.at[7])
 
     def z_weights(src, into, k, ys):
         def send(far):
@@ -181,18 +184,27 @@
         rr[r, :] = (tokens[r, own].astype(F32) * scale).astype(BF)
 
     mine = rr[0:TOK, :]
-    slot = lax.broadcasted_iota(jnp.int32, (NL, CAP, TOK), 1).astype(F32)
-    for yy in range(NY):
-        rk = rank_r[yy * NL : (yy + 1) * NL, :]
-        pick = jnp.broadcast_to(rk[:, None, :], (NL, CAP, TOK)) == slot
-        pick = pick.astype(F32).reshape(NL * CAP, TOK).astype(BF)
-        got = jnp.dot(pick, mine, preferred_element_type=F32).reshape(NL, CAP, WCOL)
-        ts[yy] = halves_down(got).astype(BF)
+    slots = [jnp.sum(jnp.where(ex == e_k, rank_r, 0.0), axis=0, keepdims=True) for e_k in (first_r, second_r)]
+    group = ids[0:1, :] // NL
+    in_group = lax.broadcasted_iota(jnp.int32, (8, TOK), 0) == group
+    place_r = jnp.dot(in_group.astype(F32).astype(BF), before, preferred_element_type=F32)
+    place_r = jnp.sum(jnp.where(in_group, place_r, 0.0), axis=0, keepdims=True)
+    spots = [(ids[k : k + 1, :] % NL).astype(F32) * CAP + slots[k] for k in range(2)]
+    spots = jnp.concatenate([*spots, jnp.zeros((6, TOK), F32)], axis=0).astype(BF)
+    row = lax.broadcasted_iota(jnp.int32, (128, TOK), 0).astype(F32)
+    for g in range(NG):
+        pick = ((row == place_r) & (group == g)).astype(F32).astype(BF)
+        got = jnp.dot(pick, mine, preferred_element_type=F32)[:GT]
+        gs[g, 0:12] = got[:, :128].reshape(12, 8, 128).astype(BF)
+        gs[g, 12:24] = got[:, 128:].reshape(12, 8, 128).astype(BF)
+        told = lax.dot_general(spots, pick, (((1,), (1,)), ((), ())), preferred_element_type=F32)
+        gs[g, 24] = told.astype(BF)
 
     with jax.named_scope("send_t"):
-        for d in (1, 3, 2):
-            y_copy(T, d).start()
-        z_tok(ts.at[my], my)
+        for i in (3, 2, 1):
+            tok_send(i).start()
+        own_group.start()
+        tok_relay(0).start()
 
     with jax.named_scope("w_far"):
         pl.semaphore_wait(far_in.at[0], 1)
@@ -215,16 +227,33 @@
         y_copy(D, d).start()
     own_down = pltpu.make_async_copy(ds.at[:, my], yd.at[:, my], loc.at[4])
     own_down.start()
+    def send_others(ds, first=0, last=NL):
+        def send(far):
+            for d in ds:
+                ys = (my + NY - d) % NY
+                copy_to(yw.at[ys, far % NL], gw.at[zz, ys], z_send.at[W], z_recv.at[W], at_z(far)).start()
+
+        if first == 0:
+            for d in ds:
+                y_copy(W, d).wait_recv()
+                ys = (my + NY - d) % NY
+                pltpu.make_async_copy(yw.at[ys, zl], gw.at[zz, ys], loc.at[W]).start()
+            send(zz + NL)
+
+        @pl.loop(max(first, 1), last)
+        def _(i):
+            send(zz + NL + i)
+            send(zz + NL - i)
+
+    with jax.named_scope("fwd_w1"):
+        send_others((1,), 0, CUT)
     with jax.named_scope("fwd_t"):
-        for d in (1, 3, 2):
-            y_copy(T, d).wait_recv()
-            ys = (my + NY - d) % NY
-            z_tok(yt.at[ys], ys)
+        for i in (1, 2, 3):
+            tok_send(i).wait_recv()
+            tok_relay(i).start()
     with jax.named_scope("fwd_w"):
-        for d in (1, 3, 2):
-            y_copy(W, d).wait_recv()
-            ys = (my + NY - d) % NY
-            z_weights(yw.at[ys], gw, W, ys)
+        send_others((1,), CUT, NL)
+        send_others((3, 2))
     with jax.named_scope("fwd_d"):
         for d in (1, 3, 2):
             y_copy(D, d).wait_recv()
@@ -232,10 +261,38 @@
         z_down(0)
         z_down(1)
 
-    ats = [
-        jnp.sum(jnp.where(ex == e_k, rank_r, 0.0), axis=0, keepdims=True) + e_k.astype(F32) * CAP
-        for e_k in (first_r, second_r)
-    ]
+
+    with jax.named_scope("w_grp"):
+        own_group.wait()
+        for i in range(4):
+            tok_relay(i).wait_recv()
+    want = (lax.broadcasted_iota(jnp.int32, (NY * CAP, 128), 0) + par * (NY * CAP)).astype(F32)
+
+    @pl.loop(0, NL)
+    def _(i):
+        v = gb[i].astype(F32)
+        told = v[24]
+        pick = ((want == told[0:1, :]) | (want == told[1:2, :])).astype(F32).astype(BF)
+        body = jnp.concatenate([v[0:12].reshape(GT, 128), v[12:24].reshape(GT, 128)], axis=1)
+        body = jnp.concatenate([body, jnp.zeros((128 - GT, WCOL), F32)], axis=0).astype(BF)
+        got = halves_down(jnp.dot(pick, body, preferred_element_type=F32).reshape(NY, CAP, WCOL)).astype(BF)
+        for yy in range(NY):
+            yt[yy, i] = got[yy]
+
+    for d in (1, 3, 2):
+        y_copy(T, d).start()
+    own_tok = pltpu.make_async_copy(yt.at[my], xa.at[mx, mc, :, my], loc.at[T])
+    own_tok.start()
+
+    def x_tok(n, d):
+        ys = (my + NY - (0, 1, 3, 2)[n]) % NY
+        rows = xa.at[mx, mc, :, ys]
+        return copy_to(rows if n else yt.at[my], rows, t_send.at[n, d], t_recv.at[n, d], {"x": (mx + d) % NX})
+
+    for d in (1, 3, 2):
+        x_tok(0, d).start()
+
+    ats = [slots[k] + e_k.astype(F32) * CAP for k, e_k in enumerate((first_r, second_r))]
     turned = jnp.concatenate([*ats, wts[...], jnp.zeros((4, TOK), F32)], axis=0).T
     cols[...] = jnp.concatenate([turned, jnp.zeros((TOK, 120), F32)], axis=1)
     outs = [
@@ -245,12 +302,11 @@
     outs[0].start()
 
     with jax.named_scope("w_ztok"):
-        wait_bytes(xa.at[0, 0, 0], loc.at[T])
-        wait_bytes(xa.at[0, 0, 0:7], z_recv.at[T])
-
-    def x_copy(ref, k, d):
-        to = (mx + d) % NX
-        return copy_to(ref.at[mx, mc], ref.at[mx, mc], x_send.at[k, d], x_recv.at[k, d], {"x": to})
+        for n, d in ((1, 1), (2, 3), (3, 2)):
+            y_copy(T, d).wait_recv()
+            for to in (1, 3, 2):
+                x_tok(n, to).start()
+        own_tok.wait()
 
     def c_copy(ref, k, d):
         who = (mx + NX - d) % NX
@@ -258,18 +314,14 @@
             ref.at[who, mc], ref.at[who, mc], x_send.at[k, NX + d], x_recv.at[k, NX + d], {"c": 1 - mc}
         )
 
-    def gather_tp(ref, k):
+    with jax.named_scope("gather_x"):
+        c_copy(xa, 0, 0).start()
         for d in (1, 3, 2):
-            x_copy(ref, k, d).start()
-        c_copy(ref, k, 0).start()
-        for d in (1, 3, 2):
-            x_copy(ref, k, d).wait_recv()
-            c_copy(ref, k, d).start()
+            for n in range(NY):
+                x_tok(n, d).wait_recv()
+            c_copy(xa, 0, d).start()
         for d in range(NX):
-            c_copy(ref, k, d).wait_recv()
-
-    with jax.named_scope("gather_x"):
-        gather_tp(xa, 0)
+            c_copy(xa, 0, d).wait_recv()
 
     @pl.loop(0, NL)
     def _(i):
@@ -285,24 +337,40 @@
         wait_bytes(gw.at[0], loc.at[W])
         wait_bytes(gw.at[0:15], z_recv.at[W])
     outs[1].start()
-    hid_rows = 128
-
-    @pl.loop(0, ROWS // hid_rows)
-    def _(i):
-        r = pl.ds(pl.multiple_of(i * hid_rows, hid_rows), hid_rows)
+    hid_rows = ROWS // 4
+
+    def x_hid(n, d):
+        at = hh.at[mx, mc, n * hid_rows : (n + 1) * hid_rows]
+        return copy_to(at, at, h_send.at[n, d], h_recv.at[n, d], {"x": (mx + d) % NX})
+
+    def c_hid(n, d):
+        at = hh.at[(mx + NX - d) % NX, mc, n * hid_rows : (n + 1) * hid_rows]
+        return copy_to(at, at, h_send.at[n, NX + d], h_recv.at[n, NX + d], {"c": 1 - mc})
+
+    for n in range(4):
+        r = slice(n * hid_rows, (n + 1) * hid_rows)
         both = jnp.dot(xr[r, :], gw[...].reshape(WIDTH, 256), preferred_element_type=F32)
         v = both[:, 0:128]
         hh[mx, mc, r, :] = (v / (1.0 + jnp.exp(-v)) * both[:, 128:256]).astype(BF)
+        for d in (2, 1, 3):
+            x_hid(n, d).start()
+        c_hid(n, 0).start()
 
     with jax.named_scope("gather_h"):
-        gather_tp(hh, 1)
+        for n in range(4):
+            for d in (1, 3, 2):
+                x_hid(n, d).wait_recv()
+                c_hid(n, d).start()
+        for n in range(4):
+            for d in range(NX):
+                c_hid(n, d).wait_recv()
 
     def back_dist(delta):
         if delta < 4:
             return -delta
         if delta > 4:
             return NL - delta
-        return NL * (zl % 2) - 4
+        return 4 - NL * (zl % 2)
 
 
     def tp_copy(h, d):
@@ -365,13 +433,19 @@
         for kind in (T, W, D):
             for d in (1, 3, 2):
                 y_copy(kind, d).wait_send()
-        wait_bytes(xa.at[0, 0, 0:7], z_send.at[T])
+        for i in range(4):
+            if i:
+                tok_send(i).wait_send()
+            tok_relay(i).wait_send()
         wait_bytes(gw.at[0:15], z_send.at[W])
-        for ref, k in ((xa, 0), (hh, 1)):
-            for d in (1, 3, 2):
-                x_copy(ref, k, d).wait_send()
-            for d in range(NX):
-                c_copy(ref, k, d).wait_send()
+        for d in (1, 3, 2):
+            for n in range(4):
+                x_hid(n, d).wait_send()
+                x_tok(n, d).wait_send()
+        for d in range(NX):
+            c_copy(xa, 0, d).wait_send()
+            for n in range(4):
+                c_hid(n, d).wait_send()
 
 
 def finish(
@@ -445,7 +519,8 @@
             pltpu.VMEM((2, NY, NL, 16, 128), BF),
             pltpu.VMEM((2, NY, NL, 16, 128), BF),
             pltpu.VMEM((2, NZ, NY, 16, 128), BF),
-            pltpu.VMEM((NY, NL, 2 * CAP, 128), BF),
+            pltpu.VMEM((NG, GT // 4 + 1, 8, 128), BF),
+            pltpu.VMEM((NL, GT // 4 + 1, 8, 128), BF),
             pltpu.VMEM((NY, NL, 2 * CAP, 128), BF),
             pltpu.VMEM((NX, NC, NL, NY, 2 * CAP, 128), BF),
             pltpu.VMEM((ROWS, WIDTH), BF),
@@ -461,10 +536,16 @@
             dma((4, NTP)),
             dma((2, 2)),
             dma((2,)),
-            dma((7,)),
+            dma((8,)),
             dma((7,)),
             dma((2,)),
             pltpu.SemaphoreType.REGULAR((2,)),
+            dma((2, 4)),
+            dma((2, 4)),
+            dma((NY, NX)),
+            dma((NY, NX)),
+            dma((4, 2 * NX)),
+            dma((4, 2 * NX)),
         ],
         compiler_params=pltpu.CompilerParams(
             collective_id=0, has_side_effects=True, vmem_limit_bytes=VMEM_MOVE * 1024 * 1024

time: 106 us -> 106 us (level)
  no operation moved by 1% of the time
where the time goes in v4:
time: 106 us; the launch traced here: 105 us
  Pallas kernels  105 us (99%)
    pallas_call x1, Pallas kernels, local(): pl.pallas_call(kernel, out_shape=(jax.ShapeDtypeStruct((NZ, NY, 32, 256),...  102 us
    pallas_call x1, Pallas kernels, local(): pl.pallas_call(finish, out_shape=(jax.ShapeDtypeStruct((NZ, NY, 32, 128),...  2.92 us

profile of v4, /device:TPU:1, one launch (start us, length us, event | category | flops | bytes accessed | tf_op | source)
XLA Modules:
  0.0 105.4 jit_solution(14655427368231657035)
XLA Ops:
  0.6 101.9 %handoff.1 = (bf16[16,4,32,256]{3,2,1,0:T(8,128)(2,1)}, bf16[8,2,2,4,16,128]{5,4,3,2,1,0:T(8,128)(2,1)}, bf16[2,4,8,3,8,128]{5,4,3,2,1,0:T(8,128)(2,1)}, f32[384,128]{1,0:T(8,128)}) custom-call(bf16[384,2048]{1,0:T(8,128)(2,1)} %tokens_in.1, s32[2,384]{1,0:T(2,128)} %bitcast.6, f32[2,384]{1,0:T(2,128)} %bitcast.7, f32[1,32]{1,0:T(1,128)} %bitcast.8, ...), custom_call_target="tpu_custom_call" | custom-call | tf_op jit(solution)/shard_map/handoff/pallas_call | solution.py:498
  102.5 2.9 %finish.1 = (bf16[16,4,32,128]{3,2,1,0:T(8,128)(2,1)}, bf16[16,4,32,128]{3,2,1,0:T(8,128)(2,1)}, bf16[2,4,16,2048]{3,2,1,0:T(8,128)(2,1)}, bf16[384,256]{1,0:T(8,128)(2,1)}) custom-call(bf16[16,4,32,256]{3,2,1,0:T(8,128)(2,1)} %get-tuple-element.12.gw_in, bf16[8,2,2,4,16,128]{5,4,3,2,1,0:T(8,128)(2,1)} %get-tuple-element.13.dn_in, ...), custom_call_target="tpu_custom_call" | custom-call | tf_op jit(solution)/shard_map/finish/pallas_call | solution.py:563
